TPU v7x, 256 devices: a whole 4x4x8 slice. The times are simulated.
256 devices in a mesh: ep: 64 (over z, y, core), tp: 4 (over x).
Axes of the slice: x: 4, y: 4, z: 8, core: 2. Of those that a mesh axis runs over, the one named last changes fastest.
Arguments:
- mixer_in: bfloat16 [32768, 4096], P(('ep', 'tp')), may hold values from -6 to 6
- mixer_gain: float32 [4096], replicated, may hold values from 0.1 to 1.9
- group_weight: bfloat16 [4, 1024, 1024], P('tp'), may hold values from -0.1875 to 0.1875
- group_scale: float32 [4, 1024], P('tp'), may hold values from 0.1 to 1.9
- expert_in: bfloat16 [32768, 4096], P(('ep', 'tp')), may hold values from -6 to 6
- expert_gain: float32 [4096], replicated, may hold values from 0.1 to 1.9
- routes: int32 [32768, 2], P('ep'), may hold values from 0 to 63, all different within a row; in each aligned block of 128 rows (0 to 127, 128 to 255, ...) at most 6 rows name the same one
- route_weight: float32 [32768, 2], P('ep'), may hold values from 0.2 to 1
- gate_weight: bfloat16 [64, 4096, 1024], P('ep', None, 'tp'), may hold values from -0.25 to 0.25
- up_weight: bfloat16 [64, 4096, 1024], P('ep', None, 'tp'), may hold values from -0.25 to 0.25
- down_weight: bfloat16 [64, 1024, 4096], P('ep', 'tp'), may hold values from -0.02734375 to 0.02734375
Outputs:
- mixed: bfloat16 [32768, 4096], P('ep', 'tp')
- expert_out: bfloat16 [32768, 4096], P(('ep', 'tp'))
Inputs may be any that keep to these rules, and one draw needn't show every extreme that they name: `routes`: each row names 2 different experts; within the rows of one device (aligned blocks of 128 rows) no expert is named more than 6 times, and that count is reached.
All inputs are finite; a program needn't handle non-finite values.
Results may differ from a plain program's by a relative error of at most 0.012.
Values may be sent and summed in bfloat16 or wider, within the bound.
A program may use at most 128 MiB of HBM per device.

v0:
```python
import jax
import jax.numpy as jnp
from jax import lax
from jax.sharding import PartitionSpec as P

WMAX = 16
TOP = 2


epsilon = 1e-06
clamp_limit = 7.0
sigmoid_slope = 1.702


def from_behind(x, axis, by):
    count = lax.axis_size(axis)
    pairs = [(i, i + by) for i in range(count) if 0 <= i + by < count]
    return lax.ppermute(x, axis, pairs)


def rms_norm(values, gain):
    widened = values.astype(jnp.float32)
    scaled = widened * lax.rsqrt(jnp.mean(widened * widened, axis=-1, keepdims=True) + epsilon)
    return (scaled * gain).astype(jnp.bfloat16)


def clamped_unit(gate_part, up_part):
    gate_part = jnp.minimum(gate_part, clamp_limit)
    up_part = jnp.clip(up_part, -clamp_limit, clamp_limit)
    return ((up_part + 1.0) * gate_part * jax.nn.sigmoid(sigmoid_slope * gate_part)).astype(
        jnp.bfloat16
    )


def slot_table(block_routes, experts, capacity):
    count = block_routes.shape[0]
    onehot = (
        block_routes[:, :, None] == jnp.arange(experts, dtype=jnp.int32)[None, None, :]
    ).astype(jnp.int32)
    per_token = jnp.sum(onehot, axis=1)
    earlier = jnp.cumsum(per_token, axis=0) - per_token
    slot_rank = jnp.sum(onehot * earlier[:, None, :], axis=2)
    matches = onehot[:, :, :, None] * (
        slot_rank[:, :, None, None] == jnp.arange(capacity, dtype=jnp.int32)[None, None, None, :]
    ).astype(jnp.int32)
    source = jnp.sum(matches * jnp.arange(count, dtype=jnp.int32)[:, None, None, None], axis=(0, 1))
    filled = jnp.sum(matches, axis=(0, 1))
    return (source, filled, slot_rank)


def shards(
    mixer_in,
    mixer_gain,
    group_weight,
    group_scale,
    expert_in,
    expert_gain,
    routes,
    route_weight,
    gate_weight,
    up_weight,
    down_weight,
):
    normed = rms_norm(mixer_in, mixer_gain)
    shard_rows = lax.all_to_all(normed, "tp", split_axis=1, concat_axis=0, tiled=True)
    length = shard_rows.shape[0]
    last_rows = shard_rows[length - (WMAX - 1) :]
    before = from_behind(last_rows, "ep", 1)
    extended = jnp.concatenate([before, shard_rows], axis=0).astype(jnp.float32)
    window = 2 << lax.axis_index("tp")
    position = lax.axis_index("ep") * length + jnp.arange(length, dtype=jnp.int32)
    prefix = jnp.concatenate(
        [jnp.zeros((1, extended.shape[1]), jnp.float32), jnp.cumsum(extended, axis=0)], axis=0
    )
    upper = prefix[WMAX:]
    lower = lax.dynamic_slice_in_dim(prefix, WMAX - window, length, 0)
    counts = jnp.minimum(position + 1, window).astype(jnp.float32)[:, None]
    pooled = ((upper - lower) / counts - extended[WMAX - 1 :]).astype(jnp.bfloat16)
    mixed = (
        jnp.dot(pooled, group_weight[0], preferred_element_type=jnp.float32) * group_scale[0]
    ).astype(jnp.bfloat16)
    expert_norm = rms_norm(expert_in, expert_gain)
    tok_count = expert_in.shape[0]
    width = expert_in.shape[1]
    experts = lax.axis_size("ep")
    capacity = max(2, 3 * tok_count * TOP // (2 * experts))
    tp_index = lax.axis_index("tp")
    own_routes = lax.dynamic_slice_in_dim(routes, tp_index * tok_count, tok_count, 0)
    own_weight = lax.dynamic_slice_in_dim(route_weight, tp_index * tok_count, tok_count, 0)
    gate_local = gate_weight[0]
    up_local = up_weight[0]
    source, filled, own_rank = slot_table(own_routes, experts, capacity)
    outgoing = expert_norm[source] * filled[:, :, None].astype(jnp.bfloat16)
    arrived = lax.all_to_all(outgoing, "ep", split_axis=0, concat_axis=0, tiled=True)
    piece = lax.all_gather(arrived.reshape(-1, width), "tp", axis=0, tiled=True)
    hidden = clamped_unit(
        jnp.dot(piece, gate_local, preferred_element_type=jnp.float32),
        jnp.dot(piece, up_local, preferred_element_type=jnp.float32),
    )
    down_local = down_weight[0]
    part_width = down_local.shape[0]
    unit_block = lax.all_to_all(hidden, "tp", split_axis=0, concat_axis=1, tiled=True)
    empty = jnp.zeros((unit_block.shape[0], width), jnp.float32)
    total = empty
    piece = lax.all_gather(down_local, "tp", axis=0, tiled=True)
    for part in range(piece.shape[0] // part_width):
        columns = lax.dynamic_slice_in_dim(unit_block, part * part_width, part_width, 1)
        partial_value = jnp.dot(
            columns,
            piece[part * part_width : (part + 1) * part_width],
            preferred_element_type=jnp.float32,
        ).astype(jnp.bfloat16)
        total = total + lax.optimization_barrier(partial_value).astype(jnp.float32)
    summed = total
    summed = summed.astype(jnp.bfloat16).reshape(experts, capacity, width)
    returned = lax.all_to_all(summed, "ep", split_axis=0, concat_axis=0, tiled=True)
    flat_rows = returned.reshape(-1, width)
    slot_index = own_routes * capacity + own_rank
    expert_sum = jnp.zeros((tok_count, width), jnp.float32)
    for choice_slot in range(TOP):
        expert_sum = (
            expert_sum
            + flat_rows[slot_index[:, choice_slot]].astype(jnp.float32)
            * own_weight[:, choice_slot : choice_slot + 1]
        )
    return (mixed, expert_sum.astype(jnp.bfloat16))


def solution(mesh):
    in_specs = (
        P(("ep", "tp"), None),
        P(),
        P("tp", None, None),
        P("tp", None),
        P(("ep", "tp"), None),
        P(),
        P("ep", None),
        P("ep", None),
        P("ep", None, "tp"),
        P("ep", None, "tp"),
        P("ep", "tp", None),
    )
    out_specs = (P("ep", "tp"), P(("ep", "tp"), None))
    return jax.shard_map(shards, mesh=mesh, in_specs=in_specs, out_specs=out_specs, check_vma=False)
```

profile of v0, /device:TPU:96, one launch (start us, length us, event | category | flops | bytes accessed | tf_op | source)
XLA Modules:
  0.0 527.5 jit_solution(16319428711208255795)
XLA Ops:
  7.2 0.8 constant_dynamic-slice_fusion.1
  8.5 0.3 multiply_reduce_fusion
  9.0 1.5 fusion.12
  10.6 1.6 fusion.14
  12.1 4.1 gather_fusion
  16.2 5.7 %reshape.101 = bf16[64,6,4096]{2,1,0:T(8,128)(2,1)} reshape(bf16[384,4096]{1,0:T(8,128)(2,1)} %gather_fusion) | data formatting | bytes 6291456 | tf_op jit(solution)/shard_map/gather | solution.py:93
  22.0 2.5 broadcast_multiply_fusion
  24.5 105.1 %all_to_all.48 = bf16[64,6,4096]{2,1,0:T(8,128)(2,1)} all-to-all(bf16[64,6,4096]{2,1,0:T(8,128)(2,1)S(1)} %broadcast_multiply_fusion), channel_id=1, replica_groups=mesh['ep'=64,'tp'=4] {'ep'}, dimensions={0} | all-to-all | bytes 6291456 | tf_op jit(solution)/shard_map/all_to_all | solution.py:94
  129.7 5.7 %reshape.97 = bf16[384,4096]{1,0:T(8,128)(2,1)} reshape(bf16[64,6,4096]{2,1,0:T(8,128)(2,1)} %all_to_all.48) | data formatting | bytes 6291456 | tf_op jit(solution)/shard_map/reshape | solution.py:95
  135.5 0.7 all-gather.6.cloned.1.call-update
  136.2 1.6 copy.27
  137.8 0.6 fusion.9
  138.4 116.5 %all-gather.4.cloned.1.call-done = bf16[1536,4096]{1,0:T(8,128)(2,1)} async-done(((bf16[384,4096]{1,0:T(8,128)(2,1)}), bf16[1536,4096]{1,0:T(8,128)(2,1)}) %all-gather.4.cloned.1.call-update) | async-done | bytes 12582928 | tf_op jit(solution)/shard_map/all_gather | solution.py:95
  254.9 7.7 %convolution_minimum_fusion = f32[1536,256]{1,0:T(8,128)S(1)} fusion(bf16[1536,4096]{1,0:T(8,128)(2,1)} %all-gather.4.cloned.1.call-done, bf16[1,4096,256]{2,1,0:T(8,128)(2,1)} %param.19), kind=kOutput, calls=%fused_computation.10 | convolution fusion | flops 3221618688 | bytes 16252928 | tf_op jit(solution)/shard_map/dot_general | solution.py:97
  262.6 1.0 copy-done.6
  263.7 0.6 copy-done.7
  264.3 4.9 fusion.5
  269.2 2.4 copy.36
  271.6 4.2 all-to-all-start.2
  275.8 1.5 fusion.11
  277.3 20.3 %all-to-all-done.2 = bf16[4,384,256]{1,2,0:T(8,128)(2,1)} async-done(((bf16[4,384,256]{1,2,0:T(8,128)(2,1)}), bf16[4,384,256]{1,2,0:T(8,128)(2,1)}, u32[]{:S(2)}, u32[]{:S(2)}) %all-to-all-start.2) | async-done | bytes 786464 | tf_op jit(solution)/shard_map/all_to_all | solution.py:102
  297.6 3.7 all-to-all-start
  301.3 61.7 %all-gather.6.cloned.1.call-done = bf16[1,1024,4096]{2,1,0:T(8,128)(2,1)} async-done(((bf16[1,256,4096]{2,1,0:T(8,128)(2,1)}), bf16[1,1024,4096]{2,1,0:T(8,128)(2,1)}) %all-gather.6.cloned.1.call-update) | async-done | bytes 8388624 | tf_op jit(solution)/shard_map/all_gather | solution.py:105
  363.0 2.8 convolution_convert_fusion.3
  365.8 3.0 convolution_convert_fusion.2
  368.8 1.9 convolution_convert_fusion.1
  370.8 1.9 convolution_convert_fusion
  372.7 4.1 add_convert_fusion
  376.8 5.7 %reshape.98 = bf16[64,6,4096]{2,1,0:T(8,128)(2,1)} reshape(bf16[384,4096]{1,0:T(8,128)(2,1)} %add_convert_fusion) | data formatting | bytes 6291456 | tf_op jit(solution)/shard_map/reshape | solution.py:115
  382.5 1.0 copy-done.3
  383.5 10.5 %all-to-all-start.3 = ((bf16[64,6,4096]{2,1,0:T(8,128)(2,1)}), bf16[64,6,4096]{2,1,0:T(8,128)(2,1)}, u32[]{:S(2)}, u32[]{:S(2)}) async-start(bf16[64,6,4096]{2,1,0:T(8,128)(2,1)} %reshape.98), calls=%async_computation.3 | async-start | bytes 8388608 | tf_op jit(solution)/shard_map/all_to_all | solution.py:116
  394.0 0.7 constant_dynamic-slice_fusion
  394.7 0.7 multiply_add_fusion
  395.4 1.5 copy.28
  396.9 2.3 collective-permute-start
  399.2 88.1 %collective-permute-done = bf16[15,1024]{1,0:T(8,128)(2,1)S(1)} collective-permute-done((bf16[15,1024]{1,0:T(8,128)(2,1)S(1)}, bf16[15,1024]{1,0:T(8,128)(2,1)S(1)}, u32[]{:S(2)}, u32[]{:S(2)}) %collective-permute-start) | collective-permute-done | bytes 30752 | tf_op jit(solution)/shard_map/ppermute | solution.py:18
  487.3 1.7 fusion.29
  489.0 0.3 pad.4
  489.3 2.6 fusion
  491.9 2.0 copy-done.1
  493.9 2.6 broadcast_add_fusion
  496.5 1.5 copy.30
  498.3 1.3 copy-done.4
  499.7 2.6 multiply_convert_fusion
  502.3 5.7 %reshape.99 = bf16[384,4096]{1,0:T(8,128)(2,1)} reshape(bf16[64,6,4096]{2,1,0:T(8,128)(2,1)} %all-to-all-done.3) | data formatting | bytes 6291456 | tf_op jit(solution)/shard_map/reshape | solution.py:117
  508.0 4.5 gather_fusion.1
  512.5 5.5 %gather_fusion.2 = bf16[128,4096]{1,0:T(8,128)(2,1)} fusion(bf16[384,4096]{1,0:T(8,128)(2,1)} %reshape.99, s32[1024]{0:T(1024)S(1)} %get-tuple-element.10), kind=kCustom, calls=%fused_computation.2 | custom fusion | bytes 2097664 | tf_op jit(solution)/shard_map/gather | solution.py:123
  518.0 2.7 add_convert_fusion.1
  (42 shorter events, 1.2 us)
Async XLA Ops:
  7.2 491.2 %copy-start = (bf16[1,1024,1024]{2,1,0:T(8,128)(2,1)S(1)}, bf16[1,1024,1024]{2,1,0:T(8,128)(2,1)}, u32[]{:S(2)}) copy-start(bf16[1,1024,1024]{2,1,0:T(8,128)(2,1)} %param.13) | copy-start | bytes 6291460
  7.2 247.7 %all-gather.4.cloned.1.call-start = ((), (), s32[]{:S(2)}) async-start(), calls=%async_computation.4 | async-start | bytes 15728640 | tf_op jit(solution)/shard_map/all_gather | solution.py:95
  135.4 227.6 %all-gather.6.cloned.1.call-start = ((), (), s32[]{:S(2)}) async-start(), calls=%async_computation.5 | async-start | bytes 10485760 | tf_op jit(solution)/shard_map/all_gather | solution.py:105
  254.9 8.8 %copy-start.6 = (bf16[1536,4096]{1,0:T(8,128)(2,1)S(1)}, bf16[1536,4096]{1,0:T(8,128)(2,1)}, u32[]{:S(2)}) copy-start(bf16[1536,4096]{1,0:T(8,128)(2,1)} %all-gather.4.cloned.1.call-done) | copy-start | bytes 37748740
  254.9 9.4 %copy-start.7 = (bf16[1,4096,256]{2,1,0:T(8,128)(2,1)S(1)}, bf16[1,4096,256]{2,1,0:T(8,128)(2,1)}, u32[]{:S(2)}) copy-start(bf16[1,4096,256]{2,1,0:T(8,128)(2,1)} %param.20) | copy-start | bytes 6291460
  269.2 6.6 %copy-start.5 = (f32[4096]{0:T(1024)S(1)}, f32[4096]{0:T(1024)}, u32[]{:S(2)}) copy-start(f32[4096]{0:T(1024)} %param.12) | copy-start | bytes 49156
  271.6 26.0 %all-to-all-start.2 = ((bf16[4,384,256]{1,2,0:T(8,128)(2,1)}), bf16[4,384,256]{1,2,0:T(8,128)(2,1)}, u32[]{:S(2)}, u32[]{:S(2)}) async-start(bf16[4,384,256]{1,2,0:T(8,128)(2,1)} %copy.36), calls=%async_computation.2 | async-start | bytes 1572864 | tf_op jit(solution)/shard_map/all_to_all | solution.py:102
  297.6 84.9 %all-to-all-start = ((bf16[128,4,1024]{0,2,1:T(8,128)(2,1)}), bf16[128,4,1024]{0,2,1:T(8,128)(2,1)S(1)}, u32[]{:S(2)}, u32[]{:S(2)}) async-start(bf16[128,4,1024]{0,2,1:T(8,128)(2,1)} %bitcast.59), calls=%async_computation | async-start | bytes 2097152 | tf_op jit(solution)/shard_map/all_to_all | solution.py:65
  363.0 5.8 %copy-start.2 = (bf16[1,1024,4096]{2,1,0:T(8,128)(2,1)S(1)}, bf16[1,1024,4096]{2,1,0:T(8,128)(2,1)}, u32[]{:S(2)}) copy-start(bf16[1,1024,4096]{2,1,0:T(8,128)(2,1)} %all-gather.6.cloned.1.call-done) | copy-start | bytes 25165828
  382.5 1.0 copy-start.3
  383.5 118.8 %all-to-all-start.3 = ((bf16[64,6,4096]{2,1,0:T(8,128)(2,1)}), bf16[64,6,4096]{2,1,0:T(8,128)(2,1)}, u32[]{:S(2)}, u32[]{:S(2)}) async-start(bf16[64,6,4096]{2,1,0:T(8,128)(2,1)} %reshape.98), calls=%async_computation.3 | async-start | bytes 8388608 | tf_op jit(solution)/shard_map/all_to_all | solution.py:116
  396.9 90.4 %collective-permute-start = (bf16[15,1024]{1,0:T(8,128)(2,1)S(1)}, bf16[15,1024]{1,0:T(8,128)(2,1)S(1)}, u32[]{:S(2)}, u32[]{:S(2)}) collective-permute-start(bf16[15,1024]{1,0:T(8,128)(2,1)S(1)} %slice.67), channel_id=1, source_target_pairs={{0,4},{4,8},{8,12},{12,16},{16,20},{20,24},{24,28},{28,32},{32,36}... | collective-permute-start | bytes 92168 | tf_op jit(solution)/shard_map/ppermute | solution.py:18
  491.9 2.0 copy-start.1
  498.0 1.6 copy-start.4
  498.1 1.6 copy-start.8
Sparse Core Ops, SparseCore 0:
  135.5 119.3 all-gather.3
  256.7 106.2 all-gather.5
where the time goes:
time: 529 us; the launch traced here: 528 us
  waiting for transfers between devices  287 us (54%)
  blocking collectives  105 us (20%)
  local copies, waits for them, and re-layouts  52.3 us (10%)
  matrix products  25 us (5%)
  other arithmetic  22.6 us (4%)
  starting transfers between devices  20.8 us (4%)
  between operations  14.3 us (3%)
    all_gather x1, waiting for transfers between devices, shards(): piece = lax.all_gather(arrived.reshape(-1, width), 'tp', axis=0, tiled=True)  117 us
    all_to_all x1, blocking collectives, shards(): lax.all_to_all(outgoing, 'ep', split_axis=0, concat_axis=0, tiled=True)  105 us
    ppermute x1, waiting for transfers between devices, from_behind(): return lax.ppermute(x, axis, pairs)  88.1 us
    all_gather x1, waiting for transfers between devices, shards(): piece = lax.all_gather(down_local, 'tp', axis=0, tiled=True)  61.7 us
    all_to_all x1, waiting for transfers between devices, shards(): lax.all_to_all(hidden, 'tp', split_axis=0, concat_axis=1, tiled=True)  20.3 us
  transfers between devices with their start and end apart: 6, of which 4 were waited for; matrix products, arithmetic and copies ran while one was open for 10% of the time, Pallas kernels for 0%

commit v1 on v0

v1 whole, which is shorter than its diff:
```python
import functools

import jax
import jax.numpy as jnp
from jax import lax
from jax.experimental import pallas as pl
from jax.experimental.pallas import tpu as pltpu
from jax.sharding import PartitionSpec as P

WMAX = 16
TOP = 2
HALO = 128
epsilon = 1e-06
clamp_limit = 7.0
sigmoid_slope = 1.702
MESH = pl.DeviceIdType.MESH
f32 = jnp.float32
bf16 = jnp.bfloat16


def aligned(value, by):
    return pl.multiple_of(value, by)


def dot(a, b):
    return jnp.dot(a, b, preferred_element_type=f32)


def layer_kernel(
    dims,
    ein, egain, min_, mgain, routes, weights, scale, perm,
    gw_hbm, g_hbm, u_hbm, d_hbm,
    mixed_hbm, out_hbm,
    en, zsend, zrecv, ysend, xs, wg, wu, wd, acc, hid,
    psend, precv, rsend, rmid, rperm, rfin, pick, mix_hi, mix_lo,
    msend, ext, gw, mixed_buf, out_buf,
    lsem, osem, ssem, zr, yr, tr, wgr, wur, wdr, pr, rr, fr, mr,
):
    NZ, NJ, TOK, D, C, CAP, FL = dims
    NC = D // C
    E = NZ * NJ
    S = E * CAP
    BJ, BZ = NJ * CAP, NZ * CAP
    GW = D // 4
    ep = lax.axis_index("ep")
    t = lax.axis_index("tp")
    z = ep // NJ
    j = ep % NJ
    t_mate = t + 1 - 2 * (t % 2)
    w_mate = 3 - t

    def remote(src, dst, send, recv, e, tt):
        return pltpu.make_async_remote_copy(
            src_ref=src, dst_ref=dst, send_sem=send, recv_sem=recv,
            device_id=(e, tt), device_id_type=MESH,
        )

    def drain(src, dst, sem):
        pltpu.make_async_copy(src, dst, sem).wait()

    barrier = pltpu.get_barrier_semaphore()

    def hello(e, tt):
        pl.semaphore_signal(barrier, inc=1, device_id=(e, tt), device_id_type=MESH)

    lax.fori_loop(1, NZ, lambda k, _: (hello(((z + k) % NZ) * NJ + j, t), 0)[1], 0)
    lax.fori_loop(1, NJ, lambda k, _: (hello(z * NJ + (j + k) % NJ, t), 0)[1], 0)
    lax.fori_loop(1, 4, lambda k, _: (hello(ep, (t + k) % 4), 0)[1], 0)

    @pl.when(ep > 0)
    def _():
        hello(ep - 1, 3)

    own_g = pltpu.make_async_copy(g_hbm.at[0], wg.at[0], lsem.at[0])
    own_u = pltpu.make_async_copy(u_hbm.at[0], wu.at[0], lsem.at[1])
    own_w = pltpu.make_async_copy(gw_hbm.at[0], gw, lsem.at[3])
    own_g.start()
    own_u.start()
    own_w.start()

    def own_d(c):
        return pltpu.make_async_copy(
            d_hbm.at[0, :, pl.ds(aligned(c * C, C), C)], wd.at[c, pl.ds(0, FL)], lsem.at[2]
        )

    def start_own_d(c, _):
        own_d(c).start()
        return 0

    lax.fori_loop(0, NC, start_own_d, 0)

    def norm_rows(src, gain, i):
        rows = pl.ds(aligned(i * 16, 16), 16)
        values = src[rows, :].astype(f32)
        mean = jnp.mean(values * values, axis=-1, keepdims=True)
        return rows, (values * lax.rsqrt(mean + epsilon) * gain[...]).astype(bf16)

    def expert_rows(i, _):
        rows, values = norm_rows(ein, egain, i)
        for c in range(NC):
            en[c, rows, :] = values[:, c * C : (c + 1) * C]
        return 0

    lax.fori_loop(0, TOK // 16, expert_rows, 0)

    own = pl.ds(aligned(t * TOK, TOK), TOK)
    r0, r1 = routes[0:1, own], routes[1:2, own]
    w0, w1 = weights[0:1, own], weights[1:2, own]
    experts = lax.broadcasted_iota(jnp.int32, (E, TOK), 0)
    is0, is1 = experts == r0, experts == r1
    named = jnp.where(is0 | is1, 1.0, 0.0).astype(bf16)
    tri = jnp.where(
        lax.broadcasted_iota(jnp.int32, (TOK, TOK), 0)
        < lax.broadcasted_iota(jnp.int32, (TOK, TOK), 1),
        1.0,
        0.0,
    ).astype(bf16)
    earlier = dot(named, tri)
    rank0 = jnp.sum(jnp.where(is0, earlier, 0.0), axis=0, keepdims=True)
    rank1 = jnp.sum(jnp.where(is1, earlier, 0.0), axis=0, keepdims=True)
    slot0 = r0 * CAP + rank0.astype(jnp.int32)
    slot1 = r1 * CAP + rank1.astype(jnp.int32)
    slots = lax.broadcasted_iota(jnp.int32, (S, TOK), 0)
    at0, at1 = slots == slot0, slots == slot1
    pick[...] = jnp.where(at0 | at1, 1.0, 0.0).astype(bf16)
    share = (jnp.where(at0, w0, 0.0) + jnp.where(at1, w1, 0.0)).T
    high = share.astype(bf16)
    mix_hi[...] = high
    mix_lo[...] = (share - high.astype(f32)).astype(bf16)

    last = ((t + 1) // 4) * (1 - (ep + 1) // E)
    pl.semaphore_wait(barrier, (NZ - 1) + (NJ - 1) + 3 + 4 * last)

    def z_copy(c, k):
        there = (z + k) % NZ
        return remote(
            zsend.at[c, there], zrecv.at[c, z], ssem.at[0], zr.at[c], there * NJ + j, t
        )

    def start_z(c, _):
        zsend[c] = dot(pick[...], en[c]).astype(bf16).reshape(NZ, BJ, C)
        zrecv[c, z] = zsend[c, z]
        lax.fori_loop(1, NZ, lambda k, _: (z_copy(c, k).start(), 0)[1], 0)
        return 0

    def wg_copy(c):
        rows = pl.ds(aligned(c * C, C), C)
        return remote(g_hbm.at[0, rows], wg.at[1, rows], ssem.at[1], wgr.at[c], ep, w_mate)

    def wu_copy(c):
        rows = pl.ds(aligned(c * C, C), C)
        return remote(u_hbm.at[0, rows], wu.at[1, rows], ssem.at[2], wur.at[c], ep, w_mate)

    def wd_copy(c):
        return remote(
            d_hbm.at[0, :, pl.ds(aligned(c * C, C), C)], wd.at[c, pl.ds(FL, FL)],
            ssem.at[3], wdr.at[c], ep, w_mate,
        )

    def start_w(c, _):
        wg_copy(c).start()
        wu_copy(c).start()
        return 0

    start_z(0, 0)
    lax.fori_loop(0, NC, start_w, 0)
    lax.fori_loop(0, NC, lambda c, _: (wd_copy(c).start(), 0)[1], 0)
    lax.fori_loop(1, NC, start_z, 0)

    def mixer_rows(i, _):
        rows, values = norm_rows(min_, mgain, i)
        for g in range(4):
            msend[g, rows, :] = values[:, g * GW : (g + 1) * GW]
        return 0

    lax.fori_loop(0, TOK // 16, mixer_rows, 0)

    def m_copy(k):
        there = (t + k) % 4
        return remote(
            msend.at[there], ext.at[pl.ds(aligned(HALO + t * TOK, 16), TOK)],
            ssem.at[4], mr.at[0], ep, there,
        )

    def halo_copy(g):
        return remote(
            msend.at[g, pl.ds(TOK - WMAX, WMAX)], ext.at[pl.ds(HALO - WMAX, WMAX)],
            ssem.at[5], mr.at[1], ep + 1, g,
        )

    lax.fori_loop(1, 4, lambda k, _: (m_copy(k).start(), 0)[1], 0)
    ext[0 : HALO - WMAX] = jnp.zeros((HALO - WMAX, GW), bf16)
    ext[pl.ds(aligned(HALO + t * TOK, 16), TOK), :] = msend[t]

    @pl.when((t == 3) & (ep < E - 1))
    def _():
        lax.fori_loop(0, 4, lambda g, _: (halo_copy(g).start(), 0)[1], 0)

    @pl.when(ep == 0)
    def _():
        ext[HALO - WMAX : HALO] = jnp.zeros((WMAX, GW), bf16)

    def clear(k, _):
        acc[k // 4, k % 4] = jnp.zeros((S, FL), f32)
        return 0

    lax.fori_loop(0, 8, clear, 0)

    def y_copy(c, k):
        there = (j + k) % NJ
        return remote(
            ysend.at[c, there], xs.at[0, c, j], ssem.at[6], yr.at[c], z * NJ + there, t
        )

    def stage_y(c):
        drain(zsend.at[c, pl.ds(0, NZ - 1)], zrecv.at[c, pl.ds(0, NZ - 1)], zr.at[c])
        moved = dot(perm[...], zrecv[c].reshape(S, C)).astype(bf16)
        ysend[c] = moved.reshape(NJ, BZ, C)
        xs[0, c, j] = ysend[c, j]
        lax.fori_loop(1, NJ, lambda k, _: (y_copy(c, k).start(), 0)[1], 0)

    def t_copy(c):
        return remote(xs.at[0, c], xs.at[1, c], ssem.at[7], tr.at[c], ep, t_mate)

    def stage_t(c):
        drain(ysend.at[c, pl.ds(0, NJ - 1)], xs.at[0, c, pl.ds(0, NJ - 1)], yr.at[c])
        t_copy(c).start()

    def stage_in(c):
        t_copy(c).wait_recv()
        wg_copy(c).wait_recv()
        wu_copy(c).wait_recv()
        rows = pl.ds(aligned(c * C, C), C)

        def half(h, _):
            x = xs[h, c].reshape(S, C)
            for part in range(2):
                acc[h, part] += dot(x, wg[part, rows, :])
                acc[h, 2 + part] += dot(x, wu[part, rows, :])
            return 0

        lax.fori_loop(0, 2, half, 0)

    def mixer():
        own_w.wait()

        def wait_peer(k, _):
            m_copy(k).wait_recv()
            return 0

        drain(msend.at[pl.ds(0, 3)], msend.at[pl.ds(0, 3)], mr.at[0])

        @pl.when(ep > 0)
        def _():
            drain(
                msend.at[0, pl.ds(0, WMAX)], ext.at[pl.ds(HALO - WMAX, WMAX)], mr.at[1]
            )

        window = jnp.left_shift(2, t)
        row = lax.broadcasted_iota(jnp.int32, (TOK, HALO + TOK), 0) + HALO
        col = lax.broadcasted_iota(jnp.int32, (TOK, HALO + TOK), 1)
        band = jnp.where((col <= row) & (col > row - window), 1.0, 0.0).astype(bf16)

        def block(b, _):
            start = aligned(b * TOK, TOK)
            sums = dot(band, ext[pl.ds(start, HALO + TOK), :])
            place = ep * (4 * TOK) + start + lax.broadcasted_iota(jnp.int32, (TOK, 1), 0)
            count = jnp.minimum(place + 1, window).astype(f32)
            center = ext[pl.ds(aligned(start + HALO, TOK), TOK), :].astype(f32)
            pooled = (sums / count - center).astype(bf16)
            mixed_buf[pl.ds(start, TOK), :] = (dot(pooled, gw[...]) * scale[...]).astype(bf16)
            return 0

        lax.fori_loop(0, 4, block, 0)
        pltpu.make_async_copy(mixed_buf, mixed_hbm, osem.at[0]).start()

    LAG = 3

    def step_in(i, _):
        @pl.when(i < NC)
        def _():
            stage_y(i)

        @pl.when(i == LAG)
        def _():
            own_g.wait()
            own_u.wait()

        @pl.when(i >= LAG)
        def _():
            stage_in(i - LAG)

        @pl.when(i < NC)
        def _():
            stage_t(i)

        @pl.when(i == 1)
        def _():
            mixer()

        return 0

    lax.fori_loop(0, NC + LAG, step_in, 0)

    def units(b, _):
        rows = pl.ds(aligned(b * 64, 64), 64)
        for h in range(2):
            for part in range(2):
                gate = jnp.minimum(acc[h, part, rows, :], clamp_limit)
                up = jnp.clip(acc[h, 2 + part, rows, :], -clamp_limit, clamp_limit)
                hid[h, rows, part * FL : (part + 1) * FL] = (
                    (up + 1.0) * gate * jax.nn.sigmoid(sigmoid_slope * gate)
                ).astype(bf16)
        return 0

    lax.fori_loop(0, S // 64, units, 0)

    def p_copy(c):
        return remote(psend.at[c], precv.at[c], ssem.at[8], pr.at[c], ep, t_mate)

    def stage_part(c):
        wd_copy(c).wait_recv()
        psend[c] = dot(hid[1], wd[c]).astype(bf16)
        p_copy(c).start()

    def r_copy(c, k):
        there = (j + k) % NJ
        return remote(
            rsend.at[c, there], rmid.at[c, j], ssem.at[9], rr.at[c], z * NJ + there, t
        )

    def stage_result(c):
        mine = dot(hid[0], wd[c])
        p_copy(c).wait_recv()
        rsend[c] = (mine + precv[c].astype(f32)).astype(bf16).reshape(NJ, BZ, C)
        rmid[c, j] = rsend[c, j]
        lax.fori_loop(1, NJ, lambda k, _: (r_copy(c, k).start(), 0)[1], 0)

    def f_copy(c, k):
        there = (z + k) % NZ
        return remote(
            rperm.at[c, there], rfin.at[c, z], ssem.at[10], fr.at[c], there * NJ + j, t
        )

    def stage_back(c):
        drain(rsend.at[c, pl.ds(0, NJ - 1)], rmid.at[c, pl.ds(0, NJ - 1)], rr.at[c])
        moved = dot(perm[...], rmid[c].reshape(S, C)).astype(bf16)
        rperm[c] = moved.reshape(NZ, BJ, C)
        rfin[c, z] = rperm[c, z]
        lax.fori_loop(1, NZ, lambda k, _: (f_copy(c, k).start(), 0)[1], 0)

    def out_copy(c):
        return pltpu.make_async_copy(
            out_buf.at[c], out_hbm.at[:, pl.ds(aligned(c * C, C), C)], osem.at[1]
        )

    def stage_out(c):
        drain(rperm.at[c, pl.ds(0, NZ - 1)], rfin.at[c, pl.ds(0, NZ - 1)], fr.at[c])
        rows = rfin[c].reshape(S, C)
        out_buf[c] = (dot(mix_hi[...], rows) + dot(mix_lo[...], rows)).astype(bf16)
        out_copy(c).start()

    lax.fori_loop(0, NC, lambda c, _: (own_d(c).wait(), 0)[1], 0)

    def step_out(i, _):
        @pl.when(i < NC)
        def _():
            stage_part(i)

        @pl.when((i >= 2) & (i < NC + 2))
        def _():
            stage_result(i - 2)

        @pl.when((i >= 3) & (i < NC + 3))
        def _():
            stage_back(i - 3)

        @pl.when(i >= 5)
        def _():
            stage_out(i - 5)

        return 0

    lax.fori_loop(0, NC + 5, step_out, 0)

    drain(zsend.at[:, pl.ds(0, NZ - 1)], zrecv.at[:, pl.ds(0, NZ - 1)], ssem.at[0])
    drain(wg.at[1], wg.at[1], ssem.at[1])
    drain(wu.at[1], wu.at[1], ssem.at[2])
    drain(wd.at[:, pl.ds(FL, FL)], wd.at[:, pl.ds(FL, FL)], ssem.at[3])
    drain(msend.at[pl.ds(0, 3)], msend.at[pl.ds(0, 3)], ssem.at[4])

    @pl.when((t == 3) & (ep < E - 1))
    def _():
        drain(msend.at[:, pl.ds(0, WMAX)], msend.at[:, pl.ds(0, WMAX)], ssem.at[5])

    drain(ysend.at[:, pl.ds(0, NJ - 1)], ysend.at[:, pl.ds(0, NJ - 1)], ssem.at[6])
    drain(xs.at[0], xs.at[1], ssem.at[7])
    drain(psend, precv, ssem.at[8])
    drain(rsend.at[:, pl.ds(0, NJ - 1)], rsend.at[:, pl.ds(0, NJ - 1)], ssem.at[9])
    drain(rperm.at[:, pl.ds(0, NZ - 1)], rperm.at[:, pl.ds(0, NZ - 1)], ssem.at[10])
    pltpu.make_async_copy(mixed_buf, mixed_hbm, osem.at[0]).wait()
    lax.fori_loop(0, NC, lambda c, _: (out_copy(c).wait(), 0)[1], 0)


def shards(
    mixer_in, mixer_gain, group_weight, group_scale, expert_in, expert_gain,
    routes, route_weight, gate_weight, up_weight, down_weight,
):
    E = lax.axis_size("ep")
    NJ = 8 if E == 64 else 2
    NZ = E // NJ
    TOK, D = expert_in.shape
    CAP = max(2, 3 * TOK * TOP // (2 * E))
    S = E * CAP
    FL = gate_weight.shape[2]
    NC = 8 if D >= 4096 else 4
    C = D // NC
    GW = D // 4
    BJ, BZ = NJ * CAP, NZ * CAP
    index = jnp.arange(S, dtype=jnp.int32)
    swapped = (index // CAP % NJ) * BZ + (index // BJ) * CAP + index % CAP
    perm = (swapped[:, None] == index[None, :]).astype(bf16)
    vmem = pl.BlockSpec(memory_space=pltpu.VMEM)
    hbm = pl.BlockSpec(memory_space=pl.ANY)
    dma = pltpu.SemaphoreType.DMA
    buf = lambda *shape: pltpu.VMEM(shape, bf16)
    return pl.pallas_call(
        functools.partial(layer_kernel, (NZ, NJ, TOK, D, C, CAP, FL)),
        out_shape=(
            jax.ShapeDtypeStruct((4 * TOK, GW), bf16),
            jax.ShapeDtypeStruct((TOK, D), bf16),
        ),
        in_specs=[vmem] * 8 + [hbm] * 4,
        out_specs=(hbm, hbm),
        scratch_shapes=[
            buf(NC, TOK, C),
            buf(NC, NZ, BJ, C), buf(NC, NZ, BJ, C), buf(NC, NJ, BZ, C),
            buf(2, NC, NJ, BZ, C),
            buf(2, D, FL), buf(2, D, FL), buf(NC, 2 * FL, C),
            pltpu.VMEM((2, 4, S, FL), f32), buf(2, S, 2 * FL),
            buf(NC, S, C), buf(NC, S, C),
            buf(NC, NJ, BZ, C), buf(NC, NJ, BZ, C),
            buf(NC, NZ, BJ, C), buf(NC, NZ, BJ, C),
            buf(S, TOK), buf(TOK, S), buf(TOK, S),
            buf(4, TOK, GW), buf(HALO + 4 * TOK, GW), buf(GW, GW), buf(4 * TOK, GW),
            buf(NC, TOK, C),
            dma((4,)), dma((2,)), dma((11,)),
            dma((NC,)), dma((NC,)), dma((NC,)), dma((NC,)), dma((NC,)), dma((NC,)),
            dma((NC,)), dma((NC,)), dma((NC,)), dma((2,)),
        ],
        compiler_params=pltpu.CompilerParams(
            collective_id=0, has_side_effects=True, vmem_limit_bytes=67043328
        ),
        name="layer",
    )(
        expert_in, expert_gain[None], mixer_in, mixer_gain[None], routes.T, route_weight.T,
        group_scale, perm, group_weight, gate_weight, up_weight, down_weight,
    )


def solution(mesh):
    in_specs = (
        P(("ep", "tp"), None),
        P(),
        P("tp", None, None),
        P("tp", None),
        P(("ep", "tp"), None),
        P(),
        P("ep", None),
        P("ep", None),
        P("ep", None, "tp"),
        P("ep", None, "tp"),
        P("ep", "tp", None),
    )
    out_specs = (P("ep", "tp"), P(("ep", "tp"), None))
    return jax.shard_map(shards, mesh=mesh, in_specs=in_specs, out_specs=out_specs, check_vma=False)
```

time: 529 us -> 320 us (0.60)
  the two profiles are of different devices: /device:TPU:96 before, /device:TPU:1 now
where the time goes in v1:
time: 320 us
  Pallas kernels  315 us (98%)
  local copies, waits for them, and re-layouts  3.32 us (1%)
    pallas_call x1, Pallas kernels, shards(): pl.pallas_call(functools.partial(layer_kernel, (NZ, NJ, TOK, D, C, CAP, F...  315 us

profile of v1, /device:TPU:1, one launch (start us, length us, event | category | flops | bytes accessed | tf_op | source)
XLA Modules:
  0.0 320.2 jit_solution(177504559386899780)
XLA Ops:
  0.6 0.8 fusion.perm
  1.5 315.4 %layer.1 = (bf16[512,1024]{1,0:T(8,128)(2,1)}, bf16[128,4096]{1,0:T(8,128)(2,1)}) custom-call(bf16[128,4096]{1,0:T(8,128)(2,1)} %ein.1, f32[1,4096]{1,0:T(1,128)} %bitcast.4, bf16[128,4096]{1,0:T(8,128)(2,1)} %min_.1, f32[1,4096]{1,0:T(1,128)} %bitcast.5, s32[2,512]{1,0:T(2,128)} %bitcast.6, f32[2,512]{1,0:T(2,128)} %bitcast.7, f32[1,1024]{1,0:T(1,128)} %scale.1, ...), custom_call_target="tpu_custom_call" | custom-call | tf_op jit(solution)/shard_map/layer/pallas_call | solution.py:427
  316.9 0.0 copy-start
  316.9 2.4 copy.15
  319.3 0.0 copy-done
  319.3 1.0 copy.16
  (1 shorter events, 0.0 us)
Async XLA Ops:
  316.9 2.4 copy-start

commit v2 on v1

--- a/solution.py
+++ b/solution.py
@@ -244,10 +244,6 @@
     def mixer():
         own_w.wait()
 
-        def wait_peer(k, _):
-            m_copy(k).wait_recv()
-            return 0
-
         drain(msend.at[pl.ds(0, 3)], msend.at[pl.ds(0, 3)], mr.at[0])
 
         @pl.when(ep > 0)
@@ -294,10 +290,6 @@
         def _():
             stage_t(i)
 
-        @pl.when(i == 1)
-        def _():
-            mixer()
-
         return 0
 
     lax.fori_loop(0, NC + LAG, step_in, 0)
@@ -374,6 +366,10 @@
         @pl.when((i >= 3) & (i < NC + 3))
         def _():
             stage_back(i - 3)
+
+        @pl.when(i == NC + 2)
+        def _():
+            mixer()
 
         @pl.when(i >= 5)
         def _():

time: 320 us -> 212 us (0.66)
  Pallas kernels: 315 us -> 207 us
    pallas_call x1, Pallas kernels: 315 us -> 207 us  [shards(): pl.pallas_call(functools.partial(layer_kernel, (NZ, NJ, TOK, D, C, CAP, F...]
where the time goes in v2:
time: 212 us
  Pallas kernels  207 us (98%)
  local copies, waits for them, and re-layouts  3.32 us (2%)
    pallas_call x1, Pallas kernels, shards(): pl.pallas_call(functools.partial(layer_kernel, (NZ, NJ, TOK, D, C, CAP, F...  207 us

profile of v2, /device:TPU:1, one launch (start us, length us, event | category | flops | bytes accessed | tf_op | source)
XLA Modules:
  0.0 211.7 jit_solution(4034382537509734090)
XLA Ops:
  0.6 0.8 fusion.perm
  1.5 206.8 %layer.1 = (bf16[512,1024]{1,0:T(8,128)(2,1)}, bf16[128,4096]{1,0:T(8,128)(2,1)}) custom-call(bf16[128,4096]{1,0:T(8,128)(2,1)} %ein.1, f32[1,4096]{1,0:T(1,128)} %bitcast.4, bf16[128,4096]{1,0:T(8,128)(2,1)} %min_.1, f32[1,4096]{1,0:T(1,128)} %bitcast.5, s32[2,512]{1,0:T(2,128)} %bitcast.6, f32[2,512]{1,0:T(2,128)} %bitcast.7, f32[1,1024]{1,0:T(1,128)} %scale.1, ...), custom_call_target="tpu_custom_call" | custom-call | tf_op jit(solution)/shard_map/layer/pallas_call | solution.py:423
  208.3 0.0 copy-start
  208.3 2.4 %copy.15 = bf16[512,1024]{1,0:T(8,128)(2,1)} copy(bf16[512,1024]{1,0:T(8,128)(2,1)} %get-tuple-element.4) | data formatting | bytes 2097152
  210.7 0.0 copy-done
  210.7 1.0 copy.16
  (1 shorter events, 0.0 us)
Async XLA Ops:
  208.3 2.4 %copy-start = (bf16[128,4096]{1,0:T(8,128)(2,1)S(1)}, bf16[128,4096]{1,0:T(8,128)(2,1)}, u32[]{:S(2)}) copy-start(bf16[128,4096]{1,0:T(8,128)(2,1)} %get-tuple-element.5) | copy-start | bytes 3145732

commit v3 on v2

--- a/solution.py
+++ b/solution.py
@@ -28,12 +28,12 @@
 
 def layer_kernel(
     dims,
-    ein, egain, min_, mgain, routes, weights, scale, perm,
-    gw_hbm, g_hbm, u_hbm, d_hbm,
+    egain, mgain, routes, weights, scale,
+    ein_hbm, min_hbm, gw_hbm, g_hbm, u_hbm, d_hbm,
     mixed_hbm, out_hbm,
     en, zsend, zrecv, ysend, xs, wg, wu, wd, acc, hid,
     psend, precv, rsend, rmid, rperm, rfin, pick, mix_hi, mix_lo,
-    msend, ext, gw, mixed_buf, out_buf,
+    ein, min_, perm, msend, relay, ext, gw, mixed_buf, out_buf,
     lsem, osem, ssem, zr, yr, tr, wgr, wur, wdr, pr, rr, fr, mr,
 ):
     NZ, NJ, TOK, D, C, CAP, FL = dims
@@ -74,6 +74,10 @@
     own_g = pltpu.make_async_copy(g_hbm.at[0], wg.at[0], lsem.at[0])
     own_u = pltpu.make_async_copy(u_hbm.at[0], wu.at[0], lsem.at[1])
     own_w = pltpu.make_async_copy(gw_hbm.at[0], gw, lsem.at[3])
+    own_e = pltpu.make_async_copy(ein_hbm, ein, lsem.at[5])
+    own_e.start()
+    own_m = pltpu.make_async_copy(min_hbm, min_, lsem.at[4])
+    own_m.start()
     own_g.start()
     own_u.start()
     own_w.start()
@@ -88,20 +92,6 @@
         return 0
 
     lax.fori_loop(0, NC, start_own_d, 0)
-
-    def norm_rows(src, gain, i):
-        rows = pl.ds(aligned(i * 16, 16), 16)
-        values = src[rows, :].astype(f32)
-        mean = jnp.mean(values * values, axis=-1, keepdims=True)
-        return rows, (values * lax.rsqrt(mean + epsilon) * gain[...]).astype(bf16)
-
-    def expert_rows(i, _):
-        rows, values = norm_rows(ein, egain, i)
-        for c in range(NC):
-            en[c, rows, :] = values[:, c * C : (c + 1) * C]
-        return 0
-
-    lax.fori_loop(0, TOK // 16, expert_rows, 0)
 
     own = pl.ds(aligned(t * TOK, TOK), TOK)
     r0, r1 = routes[0:1, own], routes[1:2, own]
@@ -128,6 +118,38 @@
     mix_hi[...] = high
     mix_lo[...] = (share - high.astype(f32)).astype(bf16)
 
+    row = lax.broadcasted_iota(jnp.int32, (S, 1), 0).astype(f32)
+    major = jnp.floor((row + 0.5) * (1.0 / BJ))
+    rest = row - BJ * major
+    minor = jnp.floor((rest + 0.5) * (1.0 / CAP))
+    source = BZ * minor + CAP * major + (rest - CAP * minor)
+    column = lax.broadcasted_iota(jnp.int32, (S, S), 1).astype(f32)
+    perm[...] = jnp.where(column == source, 1.0, 0.0).astype(bf16)
+
+    def norm_rows(src, gain, i):
+        rows = pl.ds(aligned(i * 16, 16), 16)
+        values = src[rows, :].astype(f32)
+        mean = jnp.mean(values * values, axis=-1, keepdims=True)
+        return rows, (values * lax.rsqrt(mean + epsilon) * gain[...]).astype(bf16)
+
+    def expert_rows(i, _):
+        rows, values = norm_rows(ein, egain, i)
+        for c in range(NC):
+            en[c, rows, :] = values[:, c * C : (c + 1) * C]
+        return 0
+
+    own_e.wait()
+    lax.fori_loop(0, TOK // 16, expert_rows, 0)
+
+    own_m.wait()
+    def mixer_rows(i, _):
+        rows, values = norm_rows(min_, mgain, i)
+        for g in range(4):
+            msend[g, rows, :] = values[:, g * GW : (g + 1) * GW]
+        return 0
+
+    lax.fori_loop(0, TOK // 16, mixer_rows, 0)
+
     last = ((t + 1) // 4) * (1 - (ep + 1) // E)
     pl.semaphore_wait(barrier, (NZ - 1) + (NJ - 1) + 3 + 4 * last)
 
@@ -165,22 +187,14 @@
     start_z(0, 0)
     lax.fori_loop(0, NC, start_w, 0)
     lax.fori_loop(0, NC, lambda c, _: (wd_copy(c).start(), 0)[1], 0)
-    lax.fori_loop(1, NC, start_z, 0)
-
-    def mixer_rows(i, _):
-        rows, values = norm_rows(min_, mgain, i)
-        for g in range(4):
-            msend[g, rows, :] = values[:, g * GW : (g + 1) * GW]
-        return 0
-
-    lax.fori_loop(0, TOK // 16, mixer_rows, 0)
-
-    def m_copy(k):
-        there = (t + k) % 4
-        return remote(
-            msend.at[there], ext.at[pl.ds(aligned(HALO + t * TOK, 16), TOK)],
-            ssem.at[4], mr.at[0], ep, there,
-        )
+
+    def m_rows(owner):
+        return ext.at[pl.ds(aligned(HALO + owner * TOK, 16), TOK)]
+
+    m_mate = remote(msend.at[t_mate], m_rows(t), ssem.at[4], mr.at[0], ep, t_mate)
+    m_relay = remote(msend.at[3 - t_mate], relay, ssem.at[11], mr.at[2], ep, t_mate)
+    m_weight = remote(msend.at[w_mate], m_rows(t), ssem.at[12], mr.at[3], ep, w_mate)
+    m_passed = remote(relay, m_rows(t_mate), ssem.at[13], mr.at[4], ep, w_mate)
 
     def halo_copy(g):
         return remote(
@@ -188,7 +202,8 @@
             ssem.at[5], mr.at[1], ep + 1, g,
         )
 
-    lax.fori_loop(1, 4, lambda k, _: (m_copy(k).start(), 0)[1], 0)
+    m_mate.start()
+    m_relay.start()
     ext[0 : HALO - WMAX] = jnp.zeros((HALO - WMAX, GW), bf16)
     ext[pl.ds(aligned(HALO + t * TOK, 16), TOK), :] = msend[t]
 
@@ -199,6 +214,8 @@
     @pl.when(ep == 0)
     def _():
         ext[HALO - WMAX : HALO] = jnp.zeros((WMAX, GW), bf16)
+
+    lax.fori_loop(1, NC, start_z, 0)
 
     def clear(k, _):
         acc[k // 4, k % 4] = jnp.zeros((S, FL), f32)
@@ -241,10 +258,11 @@
 
         lax.fori_loop(0, 2, half, 0)
 
-    def mixer():
+    def mixer_wait():
         own_w.wait()
-
-        drain(msend.at[pl.ds(0, 3)], msend.at[pl.ds(0, 3)], mr.at[0])
+        m_mate.wait_recv()
+        m_weight.wait_recv()
+        m_passed.wait_recv()
 
         @pl.when(ep > 0)
         def _():
@@ -252,43 +270,46 @@
                 msend.at[0, pl.ds(0, WMAX)], ext.at[pl.ds(HALO - WMAX, WMAX)], mr.at[1]
             )
 
+    def mixer_block(b):
         window = jnp.left_shift(2, t)
         row = lax.broadcasted_iota(jnp.int32, (TOK, HALO + TOK), 0) + HALO
         col = lax.broadcasted_iota(jnp.int32, (TOK, HALO + TOK), 1)
         band = jnp.where((col <= row) & (col > row - window), 1.0, 0.0).astype(bf16)
-
-        def block(b, _):
-            start = aligned(b * TOK, TOK)
-            sums = dot(band, ext[pl.ds(start, HALO + TOK), :])
-            place = ep * (4 * TOK) + start + lax.broadcasted_iota(jnp.int32, (TOK, 1), 0)
-            count = jnp.minimum(place + 1, window).astype(f32)
-            center = ext[pl.ds(aligned(start + HALO, TOK), TOK), :].astype(f32)
-            pooled = (sums / count - center).astype(bf16)
-            mixed_buf[pl.ds(start, TOK), :] = (dot(pooled, gw[...]) * scale[...]).astype(bf16)
-            return 0
-
-        lax.fori_loop(0, 4, block, 0)
-        pltpu.make_async_copy(mixed_buf, mixed_hbm, osem.at[0]).start()
-
-    LAG = 3
+        start = aligned(b * TOK, TOK)
+        sums = dot(band, ext[pl.ds(start, HALO + TOK), :])
+        place = ep * (4 * TOK) + start + lax.broadcasted_iota(jnp.int32, (TOK, 1), 0)
+        count = jnp.minimum(place + 1, window).astype(f32)
+        center = ext[pl.ds(aligned(start + HALO, TOK), TOK), :].astype(f32)
+        pooled = (sums / count - center).astype(bf16)
+        mixed_buf[pl.ds(start, TOK), :] = (dot(pooled, gw[...]) * scale[...]).astype(bf16)
+        mixed_copy(b).start()
+
+    def mixed_copy(b):
+        rows = pl.ds(aligned(b * TOK, TOK), TOK)
+        return pltpu.make_async_copy(mixed_buf.at[rows], mixed_hbm.at[rows], osem.at[0])
+
+    LAG = 4
 
     def step_in(i, _):
         @pl.when(i < NC)
         def _():
             stage_y(i)
 
+        @pl.when((i >= 1) & (i < NC + 1))
+        def _():
+            stage_t(i - 1)
+
         @pl.when(i == LAG)
         def _():
+            m_relay.wait_recv()
+            m_passed.start()
+            m_weight.start()
             own_g.wait()
             own_u.wait()
 
         @pl.when(i >= LAG)
         def _():
             stage_in(i - LAG)
-
-        @pl.when(i < NC)
-        def _():
-            stage_t(i)
 
         return 0
 
@@ -367,23 +388,30 @@
         def _():
             stage_back(i - 3)
 
-        @pl.when(i == NC + 2)
-        def _():
-            mixer()
-
-        @pl.when(i >= 5)
-        def _():
-            stage_out(i - 5)
-
-        return 0
-
-    lax.fori_loop(0, NC + 5, step_out, 0)
+        @pl.when(i == NC - 1)
+        def _():
+            mixer_wait()
+
+        @pl.when((i >= NC - 1) & (i < NC + 3))
+        def _():
+            mixer_block(i - (NC - 1))
+
+        @pl.when(i >= 6)
+        def _():
+            stage_out(i - 6)
+
+        return 0
+
+    lax.fori_loop(0, NC + 6, step_out, 0)
 
     drain(zsend.at[:, pl.ds(0, NZ - 1)], zrecv.at[:, pl.ds(0, NZ - 1)], ssem.at[0])
     drain(wg.at[1], wg.at[1], ssem.at[1])
     drain(wu.at[1], wu.at[1], ssem.at[2])
     drain(wd.at[:, pl.ds(FL, FL)], wd.at[:, pl.ds(FL, FL)], ssem.at[3])
-    drain(msend.at[pl.ds(0, 3)], msend.at[pl.ds(0, 3)], ssem.at[4])
+    m_mate.wait_send()
+    m_relay.wait_send()
+    m_weight.wait_send()
+    m_passed.wait_send()
 
     @pl.when((t == 3) & (ep < E - 1))
     def _():
@@ -394,7 +422,7 @@
     drain(psend, precv, ssem.at[8])
     drain(rsend.at[:, pl.ds(0, NJ - 1)], rsend.at[:, pl.ds(0, NJ - 1)], ssem.at[9])
     drain(rperm.at[:, pl.ds(0, NZ - 1)], rperm.at[:, pl.ds(0, NZ - 1)], ssem.at[10])
-    pltpu.make_async_copy(mixed_buf, mixed_hbm, osem.at[0]).wait()
+    lax.fori_loop(0, 4, lambda b, _: (mixed_copy(b).wait(), 0)[1], 0)
     lax.fori_loop(0, NC, lambda c, _: (out_copy(c).wait(), 0)[1], 0)
 
 
@@ -409,13 +437,10 @@
     CAP = max(2, 3 * TOK * TOP // (2 * E))
     S = E * CAP
     FL = gate_weight.shape[2]
-    NC = 8 if D >= 4096 else 4
+    NC = 16 if D >= 4096 else 4
     C = D // NC
     GW = D // 4
     BJ, BZ = NJ * CAP, NZ * CAP
-    index = jnp.arange(S, dtype=jnp.int32)
-    swapped = (index // CAP % NJ) * BZ + (index // BJ) * CAP + index % CAP
-    perm = (swapped[:, None] == index[None, :]).astype(bf16)
     vmem = pl.BlockSpec(memory_space=pltpu.VMEM)
     hbm = pl.BlockSpec(memory_space=pl.ANY)
     dma = pltpu.SemaphoreType.DMA
@@ -426,7 +451,7 @@
             jax.ShapeDtypeStruct((4 * TOK, GW), bf16),
             jax.ShapeDtypeStruct((TOK, D), bf16),
         ),
-        in_specs=[vmem] * 8 + [hbm] * 4,
+        in_specs=[vmem] * 5 + [hbm] * 6,
         out_specs=(hbm, hbm),
         scratch_shapes=[
             buf(NC, TOK, C),
@@ -438,19 +463,19 @@
             buf(NC, NJ, BZ, C), buf(NC, NJ, BZ, C),
             buf(NC, NZ, BJ, C), buf(NC, NZ, BJ, C),
             buf(S, TOK), buf(TOK, S), buf(TOK, S),
-            buf(4, TOK, GW), buf(HALO + 4 * TOK, GW), buf(GW, GW), buf(4 * TOK, GW),
+            buf(TOK, D), buf(TOK, D), buf(S, S), buf(4, TOK, GW), buf(TOK, GW), buf(HALO + 4 * TOK, GW), buf(GW, GW), buf(4 * TOK, GW),
             buf(NC, TOK, C),
-            dma((4,)), dma((2,)), dma((11,)),
+            dma((6,)), dma((2,)), dma((14,)),
             dma((NC,)), dma((NC,)), dma((NC,)), dma((NC,)), dma((NC,)), dma((NC,)),
-            dma((NC,)), dma((NC,)), dma((NC,)), dma((2,)),
+            dma((NC,)), dma((NC,)), dma((NC,)), dma((5,)),
         ],
         compiler_params=pltpu.CompilerParams(
             collective_id=0, has_side_effects=True, vmem_limit_bytes=67043328
         ),
         name="layer",
     )(
-        expert_in, expert_gain[None], mixer_in, mixer_gain[None], routes.T, route_weight.T,
-        group_scale, perm, group_weight, gate_weight, up_weight, down_weight,
+        expert_gain[None], mixer_gain[None], routes.T, route_weight.T,
+        group_scale, expert_in, mixer_in, group_weight, gate_weight, up_weight, down_weight,
     )
 
 

time: 212 us -> 198 us (0.934)
  Pallas kernels: 207 us -> 193 us
    pallas_call x1, Pallas kernels: 207 us -> 193 us  [shards(): pl.pallas_call(functools.partial(layer_kernel, (NZ, NJ, TOK, D, C, CAP, F...]
where the time goes in v3:
time: 198 us; the launch traced here: 197 us
  Pallas kernels  193 us (97%)
  local copies, waits for them, and re-layouts  3.32 us (2%)
    pallas_call x1, Pallas kernels, shards(): pl.pallas_call(functools.partial(layer_kernel, (NZ, NJ, TOK, D, C, CAP, F...  193 us

profile of v3, /device:TPU:1, one launch (start us, length us, event | category | flops | bytes accessed | tf_op | source)
XLA Modules:
  0.0 197.4 jit_solution(15859959130311850562)
XLA Ops:
  0.6 193.4 %layer.1 = (bf16[512,1024]{1,0:T(8,128)(2,1)}, bf16[128,4096]{1,0:T(8,128)(2,1)}) custom-call(f32[1,4096]{1,0:T(1,128)} %bitcast.4, f32[1,4096]{1,0:T(1,128)} %bitcast.5, s32[2,512]{1,0:T(2,128)} %bitcast.6, f32[2,512]{1,0:T(2,128)} %bitcast.7, f32[1,1024]{1,0:T(1,128)} %scale.1, bf16[128,4096]{1,0:T(8,128)(2,1)} %ein_hbm.1, bf16[128,4096]{1,0:T(8,128)(2,1)} %min_hbm.1, ...), custom_call_target="tpu_custom_call" | custom-call | tf_op jit(solution)/shard_map/layer/pallas_call | solution.py:448
  194.0 0.0 copy-start
  194.1 2.4 %copy.15 = bf16[512,1024]{1,0:T(8,128)(2,1)} copy(bf16[512,1024]{1,0:T(8,128)(2,1)} %get-tuple-element.4) | data formatting | bytes 2097152
  196.4 0.0 copy-done
  196.4 1.0 copy.16
Async XLA Ops:
  194.0 2.4 %copy-start = (bf16[128,4096]{1,0:T(8,128)(2,1)S(1)}, bf16[128,4096]{1,0:T(8,128)(2,1)}, u32[]{:S(2)}) copy-start(bf16[128,4096]{1,0:T(8,128)(2,1)} %get-tuple-element.5) | copy-start | bytes 3145732

commit v4 on v3

--- a/solution.py
+++ b/solution.py
@@ -10,6 +10,8 @@
 WMAX = 16
 TOP = 2
 HALO = 128
+CH2 = 32
+LAGS = (3, 5, 9)
 epsilon = 1e-06
 clamp_limit = 7.0
 sigmoid_slope = 1.702
@@ -36,8 +38,8 @@
     ein, min_, perm, msend, relay, ext, gw, mixed_buf, out_buf,
     lsem, osem, ssem, zr, yr, tr, wgr, wur, wdr, pr, rr, fr, mr,
 ):
-    NZ, NJ, TOK, D, C, CAP, FL = dims
-    NC = D // C
+    NZ, NJ, TOK, D, C, C2, CAP, FL = dims
+    NC, NC2 = D // C, D // C2
     E = NZ * NJ
     S = E * CAP
     BJ, BZ = NJ * CAP, NZ * CAP
@@ -55,6 +57,9 @@
             device_id=(e, tt), device_id_type=MESH,
         )
 
+    def far(k, count):
+        return count // 2 + (2 * (k % 2) - 1) * (k // 2)
+
     def drain(src, dst, sem):
         pltpu.make_async_copy(src, dst, sem).wait()
 
@@ -84,14 +89,14 @@
 
     def own_d(c):
         return pltpu.make_async_copy(
-            d_hbm.at[0, :, pl.ds(aligned(c * C, C), C)], wd.at[c, pl.ds(0, FL)], lsem.at[2]
+            d_hbm.at[0, :, pl.ds(aligned(c * C2, C2), C2)], wd.at[c, pl.ds(0, FL)], lsem.at[2]
         )
 
     def start_own_d(c, _):
         own_d(c).start()
         return 0
 
-    lax.fori_loop(0, NC, start_own_d, 0)
+    lax.fori_loop(0, NC2, start_own_d, 0)
 
     own = pl.ds(aligned(t * TOK, TOK), TOK)
     r0, r1 = routes[0:1, own], routes[1:2, own]
@@ -126,6 +131,43 @@
     column = lax.broadcasted_iota(jnp.int32, (S, S), 1).astype(f32)
     perm[...] = jnp.where(column == source, 1.0, 0.0).astype(bf16)
 
+    last = ((t + 1) // 4) * (1 - (ep + 1) // E)
+    pl.semaphore_wait(barrier, (NZ - 1) + (NJ - 1) + 3 + 4 * last)
+
+    def z_copy(c, k):
+        there = (z + far(k, NZ)) % NZ
+        return remote(
+            zsend.at[c, there], zrecv.at[c, z], ssem.at[0], zr.at[c], there * NJ + j, t
+        )
+
+    def start_z(c, _):
+        zsend[c] = dot(pick[...], en[c]).astype(bf16).reshape(NZ, BJ, C)
+        zrecv[c, z] = zsend[c, z]
+        lax.fori_loop(1, NZ, lambda k, _: (z_copy(c, k).start(), 0)[1], 0)
+        return 0
+
+    def wg_copy(c):
+        rows = pl.ds(aligned(c * C, C), C)
+        return remote(g_hbm.at[0, rows], wg.at[1, rows], ssem.at[1], wgr.at[c], ep, w_mate)
+
+    def wu_copy(c):
+        rows = pl.ds(aligned(c * C, C), C)
+        return remote(u_hbm.at[0, rows], wu.at[1, rows], ssem.at[2], wur.at[c], ep, w_mate)
+
+    def wd_copy(c):
+        return remote(
+            d_hbm.at[0, :, pl.ds(aligned(c * C2, C2), C2)], wd.at[c, pl.ds(FL, FL)],
+            ssem.at[3], wdr.at[c], ep, w_mate,
+        )
+
+    def start_w(c, _):
+        wg_copy(c).start()
+        wu_copy(c).start()
+        return 0
+
+    lax.fori_loop(0, NC, start_w, 0)
+    lax.fori_loop(0, NC2, lambda c, _: (wd_copy(c).start(), 0)[1], 0)
+
     def norm_rows(src, gain, i):
         rows = pl.ds(aligned(i * 16, 16), 16)
         values = src[rows, :].astype(f32)
@@ -141,6 +183,9 @@
     own_e.wait()
     lax.fori_loop(0, TOK // 16, expert_rows, 0)
 
+    start_z(0, 0)
+    start_z(1, 0)
+
     own_m.wait()
     def mixer_rows(i, _):
         rows, values = norm_rows(min_, mgain, i)
@@ -150,44 +195,6 @@
 
     lax.fori_loop(0, TOK // 16, mixer_rows, 0)
 
-    last = ((t + 1) // 4) * (1 - (ep + 1) // E)
-    pl.semaphore_wait(barrier, (NZ - 1) + (NJ - 1) + 3 + 4 * last)
-
-    def z_copy(c, k):
-        there = (z + k) % NZ
-        return remote(
-            zsend.at[c, there], zrecv.at[c, z], ssem.at[0], zr.at[c], there * NJ + j, t
-        )
-
-    def start_z(c, _):
-        zsend[c] = dot(pick[...], en[c]).astype(bf16).reshape(NZ, BJ, C)
-        zrecv[c, z] = zsend[c, z]
-        lax.fori_loop(1, NZ, lambda k, _: (z_copy(c, k).start(), 0)[1], 0)
-        return 0
-
-    def wg_copy(c):
-        rows = pl.ds(aligned(c * C, C), C)
-        return remote(g_hbm.at[0, rows], wg.at[1, rows], ssem.at[1], wgr.at[c], ep, w_mate)
-
-    def wu_copy(c):
-        rows = pl.ds(aligned(c * C, C), C)
-        return remote(u_hbm.at[0, rows], wu.at[1, rows], ssem.at[2], wur.at[c], ep, w_mate)
-
-    def wd_copy(c):
-        return remote(
-            d_hbm.at[0, :, pl.ds(aligned(c * C, C), C)], wd.at[c, pl.ds(FL, FL)],
-            ssem.at[3], wdr.at[c], ep, w_mate,
-        )
-
-    def start_w(c, _):
-        wg_copy(c).start()
-        wu_copy(c).start()
-        return 0
-
-    start_z(0, 0)
-    lax.fori_loop(0, NC, start_w, 0)
-    lax.fori_loop(0, NC, lambda c, _: (wd_copy(c).start(), 0)[1], 0)
-
     def m_rows(owner):
         return ext.at[pl.ds(aligned(HALO + owner * TOK, 16), TOK)]
 
@@ -215,7 +222,7 @@
     def _():
         ext[HALO - WMAX : HALO] = jnp.zeros((WMAX, GW), bf16)
 
-    lax.fori_loop(1, NC, start_z, 0)
+    lax.fori_loop(2, NC, start_z, 0)
 
     def clear(k, _):
         acc[k // 4, k % 4] = jnp.zeros((S, FL), f32)
@@ -224,7 +231,7 @@
     lax.fori_loop(0, 8, clear, 0)
 
     def y_copy(c, k):
-        there = (j + k) % NJ
+        there = (j + far(k, NJ)) % NJ
         return remote(
             ysend.at[c, there], xs.at[0, c, j], ssem.at[6], yr.at[c], z * NJ + there, t
         )
@@ -337,7 +344,7 @@
         p_copy(c).start()
 
     def r_copy(c, k):
-        there = (j + k) % NJ
+        there = (j + far(k, NJ)) % NJ
         return remote(
             rsend.at[c, there], rmid.at[c, j], ssem.at[9], rr.at[c], z * NJ + there, t
         )
@@ -345,64 +352,66 @@
     def stage_result(c):
         mine = dot(hid[0], wd[c])
         p_copy(c).wait_recv()
-        rsend[c] = (mine + precv[c].astype(f32)).astype(bf16).reshape(NJ, BZ, C)
+        rsend[c] = (mine + precv[c].astype(f32)).astype(bf16).reshape(NJ, BZ, C2)
         rmid[c, j] = rsend[c, j]
         lax.fori_loop(1, NJ, lambda k, _: (r_copy(c, k).start(), 0)[1], 0)
 
     def f_copy(c, k):
-        there = (z + k) % NZ
+        there = (z + far(k, NZ)) % NZ
         return remote(
             rperm.at[c, there], rfin.at[c, z], ssem.at[10], fr.at[c], there * NJ + j, t
         )
 
     def stage_back(c):
         drain(rsend.at[c, pl.ds(0, NJ - 1)], rmid.at[c, pl.ds(0, NJ - 1)], rr.at[c])
-        moved = dot(perm[...], rmid[c].reshape(S, C)).astype(bf16)
-        rperm[c] = moved.reshape(NZ, BJ, C)
+        moved = dot(perm[...], rmid[c].reshape(S, C2)).astype(bf16)
+        rperm[c] = moved.reshape(NZ, BJ, C2)
         rfin[c, z] = rperm[c, z]
         lax.fori_loop(1, NZ, lambda k, _: (f_copy(c, k).start(), 0)[1], 0)
 
     def out_copy(c):
         return pltpu.make_async_copy(
-            out_buf.at[c], out_hbm.at[:, pl.ds(aligned(c * C, C), C)], osem.at[1]
+            out_buf.at[c], out_hbm.at[:, pl.ds(aligned(c * C2, C2), C2)], osem.at[1]
         )
 
     def stage_out(c):
         drain(rperm.at[c, pl.ds(0, NZ - 1)], rfin.at[c, pl.ds(0, NZ - 1)], fr.at[c])
-        rows = rfin[c].reshape(S, C)
+        rows = rfin[c].reshape(S, C2)
         out_buf[c] = (dot(mix_hi[...], rows) + dot(mix_lo[...], rows)).astype(bf16)
         out_copy(c).start()
 
-    lax.fori_loop(0, NC, lambda c, _: (own_d(c).wait(), 0)[1], 0)
+    lax.fori_loop(0, NC2, lambda c, _: (own_d(c).wait(), 0)[1], 0)
+
+    A, B, O = LAGS
 
     def step_out(i, _):
-        @pl.when(i < NC)
+        @pl.when(i < NC2)
         def _():
             stage_part(i)
 
-        @pl.when((i >= 2) & (i < NC + 2))
-        def _():
-            stage_result(i - 2)
-
-        @pl.when((i >= 3) & (i < NC + 3))
-        def _():
-            stage_back(i - 3)
-
-        @pl.when(i == NC - 1)
+        @pl.when((i >= A) & (i < NC2 + A))
+        def _():
+            stage_result(i - A)
+
+        @pl.when((i >= B) & (i < NC2 + B))
+        def _():
+            stage_back(i - B)
+
+        @pl.when(i == NC2 - 2)
         def _():
             mixer_wait()
 
-        @pl.when((i >= NC - 1) & (i < NC + 3))
-        def _():
-            mixer_block(i - (NC - 1))
-
-        @pl.when(i >= 6)
-        def _():
-            stage_out(i - 6)
-
-        return 0
-
-    lax.fori_loop(0, NC + 6, step_out, 0)
+        @pl.when((i >= NC2 - 2) & (i < NC2 + 2))
+        def _():
+            mixer_block(i - (NC2 - 2))
+
+        @pl.when(i >= O)
+        def _():
+            stage_out(i - O)
+
+        return 0
+
+    lax.fori_loop(0, NC2 + O, step_out, 0)
 
     drain(zsend.at[:, pl.ds(0, NZ - 1)], zrecv.at[:, pl.ds(0, NZ - 1)], ssem.at[0])
     drain(wg.at[1], wg.at[1], ssem.at[1])
@@ -423,7 +432,7 @@
     drain(rsend.at[:, pl.ds(0, NJ - 1)], rsend.at[:, pl.ds(0, NJ - 1)], ssem.at[9])
     drain(rperm.at[:, pl.ds(0, NZ - 1)], rperm.at[:, pl.ds(0, NZ - 1)], ssem.at[10])
     lax.fori_loop(0, 4, lambda b, _: (mixed_copy(b).wait(), 0)[1], 0)
-    lax.fori_loop(0, NC, lambda c, _: (out_copy(c).wait(), 0)[1], 0)
+    lax.fori_loop(0, NC2, lambda c, _: (out_copy(c).wait(), 0)[1], 0)
 
 
 def shards(
@@ -439,6 +448,8 @@
     FL = gate_weight.shape[2]
     NC = 16 if D >= 4096 else 4
     C = D // NC
+    C2 = D // (CH2 if D >= 4096 else 4)
+    NC2 = D // C2
     GW = D // 4
     BJ, BZ = NJ * CAP, NZ * CAP
     vmem = pl.BlockSpec(memory_space=pltpu.VMEM)
@@ -446,7 +457,7 @@
     dma = pltpu.SemaphoreType.DMA
     buf = lambda *shape: pltpu.VMEM(shape, bf16)
     return pl.pallas_call(
-        functools.partial(layer_kernel, (NZ, NJ, TOK, D, C, CAP, FL)),
+        functools.partial(layer_kernel, (NZ, NJ, TOK, D, C, C2, CAP, FL)),
         out_shape=(
             jax.ShapeDtypeStruct((4 * TOK, GW), bf16),
             jax.ShapeDtypeStruct((TOK, D), bf16),
@@ -457,17 +468,17 @@
             buf(NC, TOK, C),
             buf(NC, NZ, BJ, C), buf(NC, NZ, BJ, C), buf(NC, NJ, BZ, C),
             buf(2, NC, NJ, BZ, C),
-            buf(2, D, FL), buf(2, D, FL), buf(NC, 2 * FL, C),
+            buf(2, D, FL), buf(2, D, FL), buf(NC2, 2 * FL, C2),
             pltpu.VMEM((2, 4, S, FL), f32), buf(2, S, 2 * FL),
-            buf(NC, S, C), buf(NC, S, C),
-            buf(NC, NJ, BZ, C), buf(NC, NJ, BZ, C),
-            buf(NC, NZ, BJ, C), buf(NC, NZ, BJ, C),
+            buf(NC2, S, C2), buf(NC2, S, C2),
+            buf(NC2, NJ, BZ, C2), buf(NC2, NJ, BZ, C2),
+            buf(NC2, NZ, BJ, C2), buf(NC2, NZ, BJ, C2),
             buf(S, TOK), buf(TOK, S), buf(TOK, S),
             buf(TOK, D), buf(TOK, D), buf(S, S), buf(4, TOK, GW), buf(TOK, GW), buf(HALO + 4 * TOK, GW), buf(GW, GW), buf(4 * TOK, GW),
-            buf(NC, TOK, C),
+            buf(NC2, TOK, C2),
             dma((6,)), dma((2,)), dma((14,)),
-            dma((NC,)), dma((NC,)), dma((NC,)), dma((NC,)), dma((NC,)), dma((NC,)),
-            dma((NC,)), dma((NC,)), dma((NC,)), dma((5,)),
+            dma((NC,)), dma((NC,)), dma((NC,)), dma((NC,)), dma((NC,)), dma((NC2,)),
+            dma((NC2,)), dma((NC2,)), dma((NC2,)), dma((5,)),
         ],
         compiler_params=pltpu.CompilerParams(
             collective_id=0, has_side_effects=True, vmem_limit_bytes=67043328

time: 198 us -> 192 us (0.970)
  Pallas kernels: 193 us -> 188 us
    pallas_call x1, Pallas kernels: 193 us -> 188 us  [shards(): pl.pallas_call(functools.partial(layer_kernel, (NZ, NJ, TOK, D, C, C2, CA...]
where the time goes in v4:
time: 192 us
  Pallas kernels  188 us (98%)
  local copies, waits for them, and re-layouts  3.32 us (2%)
    pallas_call x1, Pallas kernels, shards(): pl.pallas_call(functools.partial(layer_kernel, (NZ, NJ, TOK, D, C, C2, CA...  188 us

profile of v4, /device:TPU:1, one launch (start us, length us, event | category | flops | bytes accessed | tf_op | source)
XLA Modules:
  0.0 191.7 jit_solution(2614190883864272755)
XLA Ops:
  0.6 187.7 %layer.1 = (bf16[512,1024]{1,0:T(8,128)(2,1)}, bf16[128,4096]{1,0:T(8,128)(2,1)}) custom-call(f32[1,4096]{1,0:T(1,128)} %bitcast.4, f32[1,4096]{1,0:T(1,128)} %bitcast.5, s32[2,512]{1,0:T(2,128)} %bitcast.6, f32[2,512]{1,0:T(2,128)} %bitcast.7, f32[1,1024]{1,0:T(1,128)} %scale.1, bf16[128,4096]{1,0:T(8,128)(2,1)} %ein_hbm.1, bf16[128,4096]{1,0:T(8,128)(2,1)} %min_hbm.1, ...), custom_call_target="tpu_custom_call" | custom-call | tf_op jit(solution)/shard_map/layer/pallas_call | solution.py:459
  188.4 0.0 copy-start
  188.4 2.4 %copy.15 = bf16[512,1024]{1,0:T(8,128)(2,1)} copy(bf16[512,1024]{1,0:T(8,128)(2,1)} %get-tuple-element.4) | data formatting | bytes 2097152
  190.7 0.0 copy-done
  190.7 1.0 copy.16
Async XLA Ops:
  188.4 2.4 %copy-start = (bf16[128,4096]{1,0:T(8,128)(2,1)S(1)}, bf16[128,4096]{1,0:T(8,128)(2,1)}, u32[]{:S(2)}) copy-start(bf16[128,4096]{1,0:T(8,128)(2,1)} %get-tuple-element.5) | copy-start | bytes 3145732

commit v5 on v4

--- a/solution.py
+++ b/solution.py
@@ -30,11 +30,12 @@
 
 def layer_kernel(
     dims,
-    egain, mgain, routes, weights, scale,
+    egain_hbm, mgain_hbm, routes_hbm, weights_hbm, scale_hbm,
     ein_hbm, min_hbm, gw_hbm, g_hbm, u_hbm, d_hbm,
     mixed_hbm, out_hbm,
     en, zsend, zrecv, ysend, xs, wg, wu, wd, acc, hid,
     psend, precv, rsend, rmid, rperm, rfin, pick, mix_hi, mix_lo,
+    egain, mgain, routes, weights, scale,
     ein, min_, perm, msend, relay, ext, gw, mixed_buf, out_buf,
     lsem, osem, ssem, zr, yr, tr, wgr, wur, wdr, pr, rr, fr, mr,
 ):
@@ -79,6 +80,17 @@
     own_g = pltpu.make_async_copy(g_hbm.at[0], wg.at[0], lsem.at[0])
     own_u = pltpu.make_async_copy(u_hbm.at[0], wu.at[0], lsem.at[1])
     own_w = pltpu.make_async_copy(gw_hbm.at[0], gw, lsem.at[3])
+    small = [
+        pltpu.make_async_copy(a, b, lsem.at[6 + n])
+        for n, (a, b) in enumerate(
+            (
+                (routes_hbm, routes), (weights_hbm, weights), (egain_hbm, egain),
+                (mgain_hbm, mgain), (scale_hbm, scale),
+            )
+        )
+    ]
+    for copy in small:
+        copy.start()
     own_e = pltpu.make_async_copy(ein_hbm, ein, lsem.at[5])
     own_e.start()
     own_m = pltpu.make_async_copy(min_hbm, min_, lsem.at[4])
@@ -98,6 +110,8 @@
 
     lax.fori_loop(0, NC2, start_own_d, 0)
 
+    for copy in small:
+        copy.wait()
     own = pl.ds(aligned(t * TOK, TOK), TOK)
     r0, r1 = routes[0:1, own], routes[1:2, own]
     w0, w1 = weights[0:1, own], weights[1:2, own]
@@ -250,20 +264,21 @@
         drain(ysend.at[c, pl.ds(0, NJ - 1)], xs.at[0, c, pl.ds(0, NJ - 1)], yr.at[c])
         t_copy(c).start()
 
-    def stage_in(c):
+    def wait_in(c):
         t_copy(c).wait_recv()
         wg_copy(c).wait_recv()
         wu_copy(c).wait_recv()
+
+    def half_in(c, h):
         rows = pl.ds(aligned(c * C, C), C)
-
-        def half(h, _):
-            x = xs[h, c].reshape(S, C)
-            for part in range(2):
-                acc[h, part] += dot(x, wg[part, rows, :])
-                acc[h, 2 + part] += dot(x, wu[part, rows, :])
-            return 0
-
-        lax.fori_loop(0, 2, half, 0)
+        x = xs[h, c].reshape(S, C)
+        for part in range(2):
+            acc[h, part] += dot(x, wg[part, rows, :])
+            acc[h, 2 + part] += dot(x, wu[part, rows, :])
+
+    def stage_in(c):
+        wait_in(c)
+        lax.fori_loop(0, 2, lambda h, _: (half_in(c, h), 0)[1], 0)
 
     def mixer_wait():
         own_w.wait()
@@ -320,20 +335,20 @@
 
         return 0
 
-    lax.fori_loop(0, NC + LAG, step_in, 0)
-
-    def units(b, _):
-        rows = pl.ds(aligned(b * 64, 64), 64)
-        for h in range(2):
+    lax.fori_loop(0, NC + LAG - 1, step_in, 0)
+
+    def units(h):
+        def block(b, _):
+            rows = pl.ds(aligned(b * 64, 64), 64)
             for part in range(2):
                 gate = jnp.minimum(acc[h, part, rows, :], clamp_limit)
                 up = jnp.clip(acc[h, 2 + part, rows, :], -clamp_limit, clamp_limit)
                 hid[h, rows, part * FL : (part + 1) * FL] = (
                     (up + 1.0) * gate * jax.nn.sigmoid(sigmoid_slope * gate)
                 ).astype(bf16)
-        return 0
-
-    lax.fori_loop(0, S // 64, units, 0)
+            return 0
+
+        lax.fori_loop(0, S // 64, block, 0)
 
     def p_copy(c):
         return remote(psend.at[c], precv.at[c], ssem.at[8], pr.at[c], ep, t_mate)
@@ -381,11 +396,25 @@
         out_copy(c).start()
 
     lax.fori_loop(0, NC2, lambda c, _: (own_d(c).wait(), 0)[1], 0)
+    wait_in(NC - 1)
+
+    def last_half(n, _):
+        h = 1 - n
+        half_in(NC - 1, h)
+        units(h)
+
+        @pl.when(n == 0)
+        def _():
+            stage_part(0)
+
+        return 0
+
+    lax.fori_loop(0, 2, last_half, 0)
 
     A, B, O = LAGS
 
     def step_out(i, _):
-        @pl.when(i < NC2)
+        @pl.when((i >= 1) & (i < NC2))
         def _():
             stage_part(i)
 
@@ -433,6 +462,27 @@
     drain(rperm.at[:, pl.ds(0, NZ - 1)], rperm.at[:, pl.ds(0, NZ - 1)], ssem.at[10])
     lax.fori_loop(0, 4, lambda b, _: (mixed_copy(b).wait(), 0)[1], 0)
     lax.fori_loop(0, NC2, lambda c, _: (out_copy(c).wait(), 0)[1], 0)
+
+
+def handover_kernel(parts, mixed, out, mixed_to, out_to, mixed_at, out_at, isem, osem):
+    def pieces(source, target, sems):
+        rows = source.shape[0] // parts
+        return [
+            pltpu.make_async_copy(
+                source.at[pl.ds(p * rows, rows)], target.at[pl.ds(p * rows, rows)], sems.at[p]
+            )
+            for p in range(parts)
+        ]
+
+    taken = pieces(mixed, mixed_at, isem.at[0]) + pieces(out, out_at, isem.at[1])
+    given = pieces(mixed_at, mixed_to, osem.at[0]) + pieces(out_at, out_to, osem.at[1])
+    for copy in taken:
+        copy.start()
+    for copy, after in zip(taken, given):
+        copy.wait()
+        after.start()
+    for copy in given:
+        copy.wait()
 
 
 def shards(
@@ -452,17 +502,16 @@
     NC2 = D // C2
     GW = D // 4
     BJ, BZ = NJ * CAP, NZ * CAP
-    vmem = pl.BlockSpec(memory_space=pltpu.VMEM)
     hbm = pl.BlockSpec(memory_space=pl.ANY)
     dma = pltpu.SemaphoreType.DMA
     buf = lambda *shape: pltpu.VMEM(shape, bf16)
-    return pl.pallas_call(
+    mixed, out = pl.pallas_call(
         functools.partial(layer_kernel, (NZ, NJ, TOK, D, C, C2, CAP, FL)),
         out_shape=(
             jax.ShapeDtypeStruct((4 * TOK, GW), bf16),
             jax.ShapeDtypeStruct((TOK, D), bf16),
         ),
-        in_specs=[vmem] * 5 + [hbm] * 6,
+        in_specs=[hbm] * 11,
         out_specs=(hbm, hbm),
         scratch_shapes=[
             buf(NC, TOK, C),
@@ -474,9 +523,12 @@
             buf(NC2, NJ, BZ, C2), buf(NC2, NJ, BZ, C2),
             buf(NC2, NZ, BJ, C2), buf(NC2, NZ, BJ, C2),
             buf(S, TOK), buf(TOK, S), buf(TOK, S),
+            pltpu.VMEM((1, D), f32), pltpu.VMEM((1, D), f32),
+            pltpu.VMEM((2, 4 * TOK), jnp.int32), pltpu.VMEM((2, 4 * TOK), f32),
+            pltpu.VMEM((1, GW), f32),
             buf(TOK, D), buf(TOK, D), buf(S, S), buf(4, TOK, GW), buf(TOK, GW), buf(HALO + 4 * TOK, GW), buf(GW, GW), buf(4 * TOK, GW),
             buf(NC2, TOK, C2),
-            dma((6,)), dma((2,)), dma((14,)),
+            dma((11,)), dma((2,)), dma((14,)),
             dma((NC,)), dma((NC,)), dma((NC,)), dma((NC,)), dma((NC,)), dma((NC2,)),
             dma((NC2,)), dma((NC2,)), dma((NC2,)), dma((5,)),
         ],
@@ -488,6 +540,20 @@
         expert_gain[None], mixer_gain[None], routes.T, route_weight.T,
         group_scale, expert_in, mixer_in, group_weight, gate_weight, up_weight, down_weight,
     )
+    PARTS = 4
+    return pl.pallas_call(
+        functools.partial(handover_kernel, PARTS),
+        out_shape=(
+            jax.ShapeDtypeStruct((4 * TOK, GW), bf16),
+            jax.ShapeDtypeStruct((TOK, D), bf16),
+        ),
+        in_specs=[hbm] * 2,
+        out_specs=(hbm, hbm),
+        scratch_shapes=[
+            buf(4 * TOK, GW), buf(TOK, D), dma((2, PARTS)), dma((2, PARTS)),
+        ],
+        name="handover",
+    )(mixed, out)
 
 
 def solution(mesh):

time: 192 us -> 190 us (0.990)
  local copies, waits for them, and re-layouts: 3.32 us -> 0 us
    unnamed x4 -> x0, local copies, waits for them, and re-layouts: 3.32 us -> none
    pallas_call x0 -> x1, Pallas kernels: none -> 2.4 us  [shards(): pl.pallas_call(functools.partial(handover_kernel, PARTS), out_shape=(jax....]
where the time goes in v5:
time: 190 us
  Pallas kernels  189 us (99%)
    pallas_call x1, Pallas kernels, shards(): pl.pallas_call(functools.partial(layer_kernel, (NZ, NJ, TOK, D, C, C2, CA...  187 us

profile of v5, /device:TPU:1, one launch (start us, length us, event | category | flops | bytes accessed | tf_op | source)
XLA Modules:
  0.0 190.0 jit_solution(13785031156057379575)
XLA Ops:
  0.6 186.9 %layer.1 = (bf16[512,1024]{1,0:T(8,128)(2,1)}, bf16[128,4096]{1,0:T(8,128)(2,1)}) custom-call(f32[1,4096]{1,0:T(1,128)} %bitcast.4, f32[1,4096]{1,0:T(1,128)} %bitcast.5, s32[2,512]{1,0:T(2,128)} %bitcast.6, f32[2,512]{1,0:T(2,128)} %bitcast.7, f32[1,1024]{1,0:T(1,128)} %scale_hbm.1, bf16[128,4096]{1,0:T(8,128)(2,1)} %ein_hbm.1, bf16[128,4096]{1,0:T(8,128)(2,1)} %min_hbm.1, ...), custom_call_target="tpu_custom_call" | custom-call | tf_op jit(solution)/shard_map/layer/pallas_call | solution.py:508
  187.6 2.4 %handover.1 = (bf16[512,1024]{1,0:T(8,128)(2,1)}, bf16[128,4096]{1,0:T(8,128)(2,1)}) custom-call(bf16[512,1024]{1,0:T(8,128)(2,1)} %get-tuple-element.4.mixed, bf16[128,4096]{1,0:T(8,128)(2,1)} %get-tuple-element.5.out), custom_call_target="tpu_custom_call" | custom-call | tf_op jit(solution)/shard_map/handover/pallas_call | solution.py:544
